TPU v7x, 32 devices: a whole 2x2x4 slice. The times are simulated.
32 devices in a mesh: kv: 16 (over z, y, x), tp: 2 (over core).
Axes of the slice: x: 2, y: 2, z: 4, core: 2. Of those that a mesh axis runs over, the one named last changes fastest.
Arguments:
- queries: bfloat16 [4096, 1024], P('kv', 'tp'), may hold values from -4 to 4
- keys: bfloat16 [4096, 1024], P('kv', 'tp'), may hold values from -4 to 4
- values: bfloat16 [4096, 1024], P('kv', 'tp'), may hold values from -5 to 5
- log_sums: float32 [16, 4096], P('tp', 'kv'), may hold values from 5.5 to 7
- out_grad: bfloat16 [4096, 1024], P('kv', 'tp'), may hold values from -24 to 24
- chosen: int32 [32, 8], P('kv'), may hold values from -1 to 127, as said below
- normed: bfloat16 [4096, 2048], P('kv', 'tp'), may hold values from -0.23925781 to 0.23925781
Outputs:
- query_grad: bfloat16 [4096, 1024], P('kv', 'tp')
- key_grad: bfloat16 [4096, 1024], P('kv', 'tp')
- value_grad: bfloat16 [4096, 1024], P('kv', 'tp')
- weight_grad: float32 [2048, 1024], P('kv', 'tp')
Inputs may be any that keep to these rules, and one draw needn't show every extreme that they name: `chosen`: each used entry names a key block that ends at or before its query block's start; the used entries of one list are distinct. Among the lists of the 2 query blocks of one index of kv, the key blocks of any other index of kv appear as at most one distinct block; for every index from 1 on, the first query block's list names a block of the index before, and the last index's first query block's list names a block of index 0. Blocks of the own index of kv before the query block may appear freely.
All inputs are finite; a program needn't handle non-finite values.
Results may differ from a plain program's by a relative error of at most 0.008.
Values may be sent and summed in bfloat16 or wider, within the bound.
A program may use at most 64 MiB of HBM per device.

v0:
```python
from functools import partial
import jax
import jax.numpy as jnp
from jax import lax
from jax.sharding import PartitionSpec as P

QB = 128
KB = 32


def block_grads(inputs, scaling):
    query_blk, grad_blk, sums_blk, keys_sel, vals_sel, keys_own, vals_own, eligible_blocks = inputs
    span_rows = query_blk.shape[0]
    scores = (
        jnp.einsum("qhd,skhd->hqsk", query_blk, keys_sel, preferred_element_type=jnp.float32)
        * scaling
    )
    weights = jnp.where(
        eligible_blocks[None, None, :, None], jnp.exp(scores - sums_blk[:, :, None, None]), 0.0
    )
    causal = lax.broadcasted_iota(jnp.int32, (span_rows, span_rows), 0) >= lax.broadcasted_iota(
        jnp.int32, (span_rows, span_rows), 1
    )
    own_scores = (
        jnp.einsum("qhd,khd->hqk", query_blk, keys_own, preferred_element_type=jnp.float32)
        * scaling
    )
    own_weights = jnp.where(causal[None], jnp.exp(own_scores - sums_blk[:, :, None]), 0.0)
    weights_low = weights.astype(jnp.bfloat16)
    own_low = own_weights.astype(jnp.bfloat16)
    attended = jnp.einsum(
        "hqsk,skhd->qhd", weights_low, vals_sel, preferred_element_type=jnp.float32
    )
    attended = attended + jnp.einsum(
        "hqk,khd->qhd", own_low, vals_own, preferred_element_type=jnp.float32
    )
    deltas = jnp.sum(grad_blk.astype(jnp.float32) * attended, axis=-1).T
    dots_sel = jnp.einsum("qhd,skhd->hqsk", grad_blk, vals_sel, preferred_element_type=jnp.float32)
    own_dots = jnp.einsum("qhd,khd->hqk", grad_blk, vals_own, preferred_element_type=jnp.float32)
    slopes = (weights * (dots_sel - deltas[:, :, None, None])).astype(jnp.bfloat16)
    own_slopes = (own_weights * (own_dots - deltas[:, :, None])).astype(jnp.bfloat16)
    query_part = jnp.einsum("hqsk,skhd->qhd", slopes, keys_sel, preferred_element_type=jnp.float32)
    query_part = scaling * (
        query_part
        + jnp.einsum("hqk,khd->qhd", own_slopes, keys_own, preferred_element_type=jnp.float32)
    )
    key_terms = scaling * jnp.einsum(
        "hqsk,qhd->skhd", slopes, query_blk, preferred_element_type=jnp.float32
    )
    value_terms = jnp.einsum(
        "hqsk,qhd->skhd", weights_low, grad_blk, preferred_element_type=jnp.float32
    )
    own_key_terms = scaling * jnp.einsum(
        "hqk,qhd->khd", own_slopes, query_blk, preferred_element_type=jnp.float32
    )
    own_value_terms = jnp.einsum(
        "hqk,qhd->khd", own_low, grad_blk, preferred_element_type=jnp.float32
    )
    return (query_part.astype(jnp.bfloat16), key_terms, value_terms, own_key_terms, own_value_terms)


def body(queries, keys, values, log_sums, out_grad, chosen, normed):
    devices = lax.axis_size("kv")
    myself = lax.axis_index("kv")
    rows_here, columns = queries.shape
    head_count = log_sums.shape[0]
    head_size = columns // head_count
    query_blocks = rows_here // QB
    key_blocks = rows_here // KB
    selected = chosen.shape[1]
    groups = 1
    slot_count = devices * groups
    owners = chosen // key_blocks
    offsets = chosen % key_blocks
    eligible_blocks = chosen >= 0
    remote = eligible_blocks & (owners != myself)
    slot_ids = owners * groups
    matches = remote[:, :, None] & (
        slot_ids[:, :, None] == jnp.arange(slot_count, dtype=jnp.int32)[None, None, :]
    )
    wanted = jnp.max(jnp.where(matches, offsets[:, :, None] + 1, 0), axis=(0, 1))
    requested = lax.all_to_all(
        wanted.reshape(devices, groups), "kv", split_axis=0, concat_axis=0, tiled=True
    ).reshape(-1)
    live_request = requested > 0
    picked = jnp.clip(requested - 1, 0, key_blocks - 1)
    key_table = keys.reshape(key_blocks, KB, columns)
    value_table = values.reshape(key_blocks, KB, columns)
    zero_block = jnp.zeros((), keys.dtype)
    outgoing_keys = jnp.where(live_request[:, None, None], key_table[picked], zero_block).reshape(
        devices, groups, KB, columns
    )
    outgoing_values = jnp.where(
        live_request[:, None, None], value_table[picked], zero_block
    ).reshape(devices, groups, KB, columns)
    fetched_keys, fetched_values = (
        lax.all_to_all(outgoing_keys, "kv", split_axis=0, concat_axis=0, tiled=True),
        lax.all_to_all(outgoing_values, "kv", split_axis=0, concat_axis=0, tiled=True),
    )
    all_keys = jnp.concatenate([fetched_keys.reshape(slot_count, KB, columns), key_table], axis=0)
    all_values = jnp.concatenate(
        [fetched_values.reshape(slot_count, KB, columns), value_table], axis=0
    )
    table_ids = jnp.where(remote, slot_ids, jnp.where(eligible_blocks, slot_count + offsets, 0))
    keys_sel = all_keys[table_ids].reshape(query_blocks, selected, KB, head_count, head_size)
    vals_sel = all_values[table_ids].reshape(query_blocks, selected, KB, head_count, head_size)
    block_shape = (query_blocks, QB, head_count, head_size)
    inputs = (
        queries.reshape(block_shape),
        out_grad.reshape(block_shape),
        log_sums.reshape(head_count, query_blocks, QB).transpose(1, 0, 2),
        keys_sel,
        vals_sel,
        keys.reshape(block_shape),
        values.reshape(block_shape),
        eligible_blocks,
    )
    query_part, key_terms, value_terms, own_key_terms, own_value_terms = lax.map(
        partial(block_grads, scaling=head_size ** (-0.5)), inputs
    )
    routes = (
        table_ids.reshape(-1)[:, None]
        == jnp.arange(slot_count + key_blocks, dtype=jnp.int32)[None, :]
    ) & eligible_blocks.reshape(-1)[:, None]
    stacked_terms = jnp.stack(
        [key_terms.reshape(-1, KB * columns), value_terms.reshape(-1, KB * columns)]
    )
    routed = jnp.einsum(
        "ab,xac->xbc", routes.astype(jnp.float32), stacked_terms, precision=lax.Precision.HIGHEST
    )
    back_keys = routed[0, :slot_count].reshape(devices, groups, KB, columns)
    back_values = routed[1, :slot_count].reshape(devices, groups, KB, columns)
    returned_keys, returned_values = (
        lax.all_to_all(back_keys, "kv", split_axis=0, concat_axis=0, tiled=True),
        lax.all_to_all(back_values, "kv", split_axis=0, concat_axis=0, tiled=True),
    )
    matched = (
        ((requested - 1)[:, None] == jnp.arange(key_blocks, dtype=jnp.int32)[None, :])
        & live_request[:, None]
    ).astype(jnp.float32)
    stacked_back = jnp.stack(
        [
            returned_keys.reshape(slot_count, KB * columns),
            returned_values.reshape(slot_count, KB * columns),
        ]
    )
    arrived = jnp.einsum("ab,xac->xbc", matched, stacked_back, precision=lax.Precision.HIGHEST)
    totals = arrived + routed[:, slot_count:]
    key_grad = (
        totals[0].reshape(rows_here, columns) + own_key_terms.reshape(rows_here, columns)
    ).astype(jnp.bfloat16)
    value_grad = (
        totals[1].reshape(rows_here, columns) + own_value_terms.reshape(rows_here, columns)
    ).astype(jnp.bfloat16)
    features_all = lax.all_gather(normed, "tp", axis=1, tiled=True)
    weight_grad = lax.psum_scatter(
        lax.dot_general(
            features_all, value_grad, (((0,), (0,)), ((), ())), preferred_element_type=jnp.float32
        ),
        "kv",
        scatter_dimension=0,
        tiled=True,
    )
    return (query_part.reshape(rows_here, columns), key_grad, value_grad, weight_grad)


def solution(mesh):
    in_specs = (
        P("kv", "tp"),
        P("kv", "tp"),
        P("kv", "tp"),
        P("tp", "kv"),
        P("kv", "tp"),
        P("kv", None),
        P("kv", "tp"),
    )
    out_specs = (P("kv", "tp"), P("kv", "tp"), P("kv", "tp"), P("kv", "tp"))
    return jax.shard_map(body, mesh=mesh, in_specs=in_specs, out_specs=out_specs, check_vma=False)
```

profile of v0, /device:TPU:0, one launch (start us, length us, event | category | flops | bytes accessed | tf_op | source)
XLA Modules:
  0.0 302.4 jit_solution(817550221960606764)
XLA Ops:
  7.2 0.7 compare_select_fusion
  8.1 15.4 %all_to_all.29 = s32[16,1,1]{2,1,0:T(1,128)S(1)} all-to-all(s32[16,1,1]{2,1,0:T(1,128)S(1)} %copy.86), channel_id=1, replica_groups=mesh['kv'=16,'tp'=2] {'kv'}, dimensions={0} | all-to-all | bytes 128 | tf_op jit(solution)/shard_map/all_to_all | solution.py:82
  23.5 0.7 add_reduce_fusion
  24.2 1.5 gather_fusion.2
  25.7 1.5 gather_fusion
  27.7 0.9 bitcast_select_fusion
  28.6 16.8 %all_to_all.30 = bf16[16,1,32,512]{3,2,1,0:T(8,128)(2,1)S(1)} all-to-all(bf16[16,1,32,512]{3,2,1,0:T(8,128)(2,1)S(1)} %get-tuple-element.203), channel_id=1, replica_groups=mesh['kv'=16,'tp'=2] {'kv'}, dimensions={0} | all-to-all | bytes 1048576 | tf_op jit(solution)/shard_map/all_to_all | solution.py:97
  45.3 3.9 %all-to-all-start.2 = ((bf16[16,1,32,512]{3,2,1,0:T(8,128)(2,1)}), bf16[16,1,32,512]{3,2,1,0:T(8,128)(2,1)S(1)}, u32[]{:S(2)}, u32[]{:S(2)}) async-start(bf16[16,1,32,512]{3,2,1,0:T(8,128)(2,1)} %get-tuple-element.202), calls=%async_computation.2 | async-start | bytes 1048576 | tf_op jit(solution)/shard_map/all_to_all | solution.py:98
  49.4 1.1 reshape.196
  50.9 1.1 reshape.194
  52.0 1.3 copy.92
  53.3 1.1 reshape.195
  54.4 1.3 copy.93
  55.7 2.0 copy.95
  57.7 1.0 copy.96
  58.9 0.6 gather_fusion.1
  59.5 0.5 reshape.132
  60.0 3.3 %all-to-all-done.2 = bf16[16,1,32,512]{3,2,1,0:T(8,128)(2,1)S(1)} async-done(((bf16[16,1,32,512]{3,2,1,0:T(8,128)(2,1)}), bf16[16,1,32,512]{3,2,1,0:T(8,128)(2,1)S(1)}, u32[]{:S(2)}, u32[]{:S(2)}) %all-to-all-start.2) | async-done | bytes 524320 | tf_op jit(solution)/shard_map/all_to_all | solution.py:98
  63.4 0.6 gather_fusion.3
  64.5 56.6 %while.18 = (s32[]{:T(128)}, bf16[2,128,8,64]{1,3,2,0:T(8,128)(2,1)}, f32[2,8,32,8,64]{4,3,2,1,0:T(8,128)}, f32[2,8,32,8,64]{4,3,2,1,0:T(8,128)}, f32[2,128,8,64...) while((s32[]{:T(128)}, ...), condition=%wide.region_3.4_spmd, body=%wide.region_1.3_spmd.sunk | while | flops 306330624 | bytes 43585888 | solution.py:118
  66.0 1.2 fusion.157
  67.2 1.2 fusion.158
  69.1 1.2 fusion.159
  70.4 1.9 fusion.160
  72.9 0.9 copy-done.5
  73.8 0.7 copy-done.2
  74.5 1.9 copy_dynamic-update-slice_fusion.3
  76.7 1.1 copy-done.3
  77.8 0.6 copy-done.6
  78.4 7.1 %dynamic_update_slice.27 = f32[2,128,8,64]{1,0,3,2:T(2,128)} dynamic-update-slice(f32[2,128,8,64]{1,0,3,2:T(2,128)} %get-tuple-element.313, f32[1,128,8,64]{1,0,3,2:T(1,128)S(1)} %bitcast.262, s32[]{:T(128)S(6)} %copy.169, s32[]{:T(128)} %constant.73.clone.1..sunk, s32[]{:T(128)} %constant.73.clone.1..sunk, s32[]{:T(128)} %constant.73.clone.1..sunk) | dynamic-update-slice | bytes 524292 | tf_op jit(solution)/shard_map/while/body/jit(dynamic_update_index_in_dim)/dynamic_update_slice | solution.py:118
  85.7 7.1 %dynamic_update_slice.28 = f32[2,128,8,64]{1,0,3,2:T(2,128)} dynamic-update-slice(f32[2,128,8,64]{1,0,3,2:T(2,128)} %get-tuple-element.314, f32[1,128,8,64]{1,0,3,2:T(1,128)S(1)} %bitcast.261, s32[]{:T(128)S(6)} %copy.169, s32[]{:T(128)} %constant.73.clone.1..sunk, s32[]{:T(128)} %constant.73.clone.1..sunk, s32[]{:T(128)} %constant.73.clone.1..sunk) | dynamic-update-slice | bytes 524292 | tf_op jit(solution)/shard_map/while/body/jit(dynamic_update_index_in_dim)/dynamic_update_slice | solution.py:118
  94.3 1.2 fusion.157
  95.6 1.2 fusion.158
  97.5 1.2 fusion.159
  98.7 1.9 fusion.160
  101.3 0.9 copy-done.5
  102.1 0.7 copy-done.2
  102.8 1.9 copy_dynamic-update-slice_fusion.3
  105.0 1.1 copy-done.3
  106.1 0.6 copy-done.6
  106.7 7.1 %dynamic_update_slice.27 = f32[2,128,8,64]{1,0,3,2:T(2,128)} dynamic-update-slice(f32[2,128,8,64]{1,0,3,2:T(2,128)} %get-tuple-element.313, f32[1,128,8,64]{1,0,3,2:T(1,128)S(1)} %bitcast.262, s32[]{:T(128)S(6)} %copy.169, s32[]{:T(128)} %constant.73.clone.1..sunk, s32[]{:T(128)} %constant.73.clone.1..sunk, s32[]{:T(128)} %constant.73.clone.1..sunk) | dynamic-update-slice | bytes 524292 | tf_op jit(solution)/shard_map/while/body/jit(dynamic_update_index_in_dim)/dynamic_update_slice | solution.py:118
  114.0 7.1 %dynamic_update_slice.28 = f32[2,128,8,64]{1,0,3,2:T(2,128)} dynamic-update-slice(f32[2,128,8,64]{1,0,3,2:T(2,128)} %get-tuple-element.314, f32[1,128,8,64]{1,0,3,2:T(1,128)S(1)} %bitcast.261, s32[]{:T(128)S(6)} %copy.169, s32[]{:T(128)} %constant.73.clone.1..sunk, s32[]{:T(128)} %constant.73.clone.1..sunk, s32[]{:T(128)} %constant.73.clone.1..sunk) | dynamic-update-slice | bytes 524292 | tf_op jit(solution)/shard_map/while/body/jit(dynamic_update_index_in_dim)/dynamic_update_slice | solution.py:118
  121.2 3.3 %stack_reshape.13 = f32[1,16,16384]{2,1,0:T(8,128)} reshape(f32[2,8,32,8,64]{4,3,2,1,0:T(8,128)} %get-tuple-element.82) | data formatting | bytes 2097152 | tf_op jit(solution)/shard_map/stack;reshape | solution.py:125
  124.5 1.6 stack_reshape.12
  126.1 3.1 %convolution_bitcast_fusion.2 = f32[2,24,16384]{2,1,0:T(8,128)S(1)} fusion(f32[1,16,16384]{2,1,0:T(8,128)} %stack_reshape.13, f32[1,16,16384]{2,1,0:T(8,128)} %stack_reshape.12, s32[16]{0:T(128)S(1)} %eq.46, pred[16]{0:T(512)(128)(4,1)S(1)} %and.45), kind=kOutput, calls=%fused_computation.80 | convolution fusion | flops 151520000 | bytes 5242960 | tf_op jit(solution)/shard_map/ab,xac->xbc/dot_general | solution.py:128
  129.2 1.1 fusion.82
  130.3 1.6 copy.133
  131.9 4.3 %all-to-all-start.4 = ((f32[16,1,32,512]{3,2,1,0:T(8,128)}), f32[16,1,32,512]{3,2,1,0:T(8,128)}, u32[]{:S(2)}, u32[]{:S(2)}) async-start(f32[16,1,32,512]{3,2,1,0:T(8,128)} %bitcast.264), calls=%async_computation.4 | async-start | bytes 2097152 | tf_op jit(solution)/shard_map/all_to_all | solution.py:135
  136.3 2.8 copy.132
  139.1 20.0 %all-to-all-done.4 = f32[16,1,32,512]{3,2,1,0:T(8,128)} async-done(((f32[16,1,32,512]{3,2,1,0:T(8,128)}), f32[16,1,32,512]{3,2,1,0:T(8,128)}, u32[]{:S(2)}, u32[]{:S(2)}) %all-to-all-start.4) | async-done | bytes 1048608 | tf_op jit(solution)/shard_map/all_to_all | solution.py:135
  159.1 6.1 %all-to-all-start.3 = ((f32[16,1,32,512]{3,2,1,0:T(8,128)}), f32[16,1,32,512]{3,2,1,0:T(8,128)}, u32[]{:S(2)}, u32[]{:S(2)}) async-start(f32[16,1,32,512]{3,2,1,0:T(8,128)} %bitcast.263), calls=%async_computation.3 | async-start | bytes 2097152 | tf_op jit(solution)/shard_map/all_to_all | solution.py:134
  165.2 0.7 all-gather.2.cloned.1.call-update
  166.0 2.4 stack_reshape.15
  168.4 19.8 %all-to-all-done.3 = f32[16,1,32,512]{3,2,1,0:T(8,128)} async-done(((f32[16,1,32,512]{3,2,1,0:T(8,128)}), f32[16,1,32,512]{3,2,1,0:T(8,128)}, u32[]{:S(2)}, u32[]{:S(2)}) %all-to-all-start.3) | async-done | bytes 1048608 | tf_op jit(solution)/shard_map/all_to_all | solution.py:134
  188.1 2.4 stack_reshape.14
  190.5 2.3 fusion.59
  193.3 0.6 copy-done.8
  194.0 3.9 %convolution_bitcast_fusion.4 = f32[2048,512]{0,1:T(8,128)} fusion(bf16[256,512]{0,1:T(8,128)(2,1)S(1)} %fusion.66, bf16[256,2048]{1,0:T(8,128)(2,1)} %all-gather.2.cloned.1.call-done), kind=kOutput, calls=%fused_computation.83 | convolution fusion | flops 536870912 | bytes 5505024 | tf_op jit(solution)/shard_map/dot_general | solution.py:157
  198.0 1.3 copy.120
  199.3 1.0 reshape.198
  200.3 0.8 copy.108
  201.5 0.8 copy.107
  202.4 91.4 %reduce-scatter.2.cloned.1.call-done = f32[128,512]{0,1:T(8,128)} async-done(((f32[2048,512]{0,1:T(8,128)}), f32[128,512]{0,1:T(8,128)}) %reduce-scatter.2.cloned.1.call-update) | async-done | bytes 262160 | tf_op jit(solution)/shard_map/reduce_scatter | solution.py:156
  293.8 1.8 copy.109
  (89 shorter events, 9.0 us)
Async XLA Ops:
  27.6 21.7 %copy-start.1 = (bf16[256,512]{1,0:T(8,128)(2,1)S(1)}, bf16[256,512]{1,0:T(8,128)(2,1)}, u32[]{:S(2)}) copy-start(bf16[256,512]{1,0:T(8,128)(2,1)} %param.11) | copy-start | bytes 786436
  27.6 22.8 %copy-start = (bf16[256,512]{1,0:T(8,128)(2,1)S(1)}, bf16[256,512]{1,0:T(8,128)(2,1)}, u32[]{:S(2)}) copy-start(bf16[256,512]{1,0:T(8,128)(2,1)} %param.10) | copy-start | bytes 786436
  28.6 22.3 %copy-start.9 = (bf16[256,512]{1,0:T(8,128)(2,1)S(1)}, bf16[256,512]{1,0:T(8,128)(2,1)}, u32[]{:S(2)}) copy-start(bf16[256,512]{1,0:T(8,128)(2,1)} %param.9) | copy-start | bytes 786436
  45.3 7.9 %copy-start.10 = (bf16[256,512]{1,0:T(8,128)(2,1)S(1)}, bf16[256,512]{1,0:T(8,128)(2,1)}, u32[]{:S(2)}) copy-start(bf16[256,512]{1,0:T(8,128)(2,1)} %param.13) | copy-start | bytes 786436
  45.3 18.0 %all-to-all-start.2 = ((bf16[16,1,32,512]{3,2,1,0:T(8,128)(2,1)}), bf16[16,1,32,512]{3,2,1,0:T(8,128)(2,1)S(1)}, u32[]{:S(2)}, u32[]{:S(2)}) async-start(bf16[16,1,32,512]{3,2,1,0:T(8,128)(2,1)} %get-tuple-element.202), calls=%async_computation.2 | async-start | bytes 1048576 | tf_op jit(solution)/shard_map/all_to_all | solution.py:98
  63.3 1.2 copy-start.11
  72.2 1.6 copy-start.5
  72.5 2.0 copy-start.2
  76.4 1.3 copy-start.3
  76.4 1.9 copy-start.6
  100.5 1.6 copy-start.5
  100.8 2.0 copy-start.2
  104.7 1.3 copy-start.3
  104.7 1.9 copy-start.6
  121.2 3.3 %copy-start.4 = (f32[2,8,32,8,64]{4,3,2,1,0:T(8,128)S(1)}, f32[2,8,32,8,64]{4,3,2,1,0:T(8,128)}, u32[]{:S(2)}) copy-start(f32[2,8,32,8,64]{4,3,2,1,0:T(8,128)} %get-tuple-element.81) | copy-start | bytes 3145732
  131.9 27.1 %all-to-all-start.4 = ((f32[16,1,32,512]{3,2,1,0:T(8,128)}), f32[16,1,32,512]{3,2,1,0:T(8,128)}, u32[]{:S(2)}, u32[]{:S(2)}) async-start(f32[16,1,32,512]{3,2,1,0:T(8,128)} %bitcast.264), calls=%async_computation.4 | async-start | bytes 2097152 | tf_op jit(solution)/shard_map/all_to_all | solution.py:135
  159.1 29.1 %all-to-all-start.3 = ((f32[16,1,32,512]{3,2,1,0:T(8,128)}), f32[16,1,32,512]{3,2,1,0:T(8,128)}, u32[]{:S(2)}, u32[]{:S(2)}) async-start(f32[16,1,32,512]{3,2,1,0:T(8,128)} %bitcast.263), calls=%async_computation.3 | async-start | bytes 2097152 | tf_op jit(solution)/shard_map/all_to_all | solution.py:134
  165.2 28.9 %all-gather.2.cloned.1.call-start = ((), (), s32[]{:S(2)}) async-start(), calls=%async_computation.6 | async-start | bytes 1572864 | tf_op jit(solution)/shard_map/all_gather | solution.py:155
  165.9 127.9 %reduce-scatter.2.cloned.1.call-start = ((), (), s32[]{:S(2)}) async-start(), calls=%async_computation.7 | async-start | bytes 4456448 | tf_op jit(solution)/shard_map/reduce_scatter | solution.py:156
  192.9 1.0 copy-start.8
  197.9 3.5 %copy-start.7 = (f32[2,128,8,64]{1,0,3,2:T(2,128)S(1)}, f32[2,128,8,64]{1,0,3,2:T(2,128)}, u32[]{:S(2)}) copy-start(f32[2,128,8,64]{1,0,3,2:T(2,128)} %get-tuple-element.83) | copy-start | bytes 1572868
Sparse Core Ops, SparseCore 0:
  167.5 10.2 all-gather.1
  198.1 95.6 reduce-scatter.1
where the time goes:
time: 305 us; the launch traced here: 302 us
  waiting for transfers between devices  135 us (44%)
  local copies, waits for them, and re-layouts  76.8 us (25%)
  blocking collectives  32.2 us (11%)
  matrix products  24.7 us (8%)
  starting transfers between devices  14.5 us (5%)
  between operations  14.3 us (5%)
  other arithmetic  4.52 us (1%)
    reduce_scatter x1, waiting for transfers between devices, body(): lax.psum_scatter(lax.dot_general(features_all, value_grad, (((0,), (0,)),...  91.4 us
    dynamic_update_slice x6, local copies, waits for them, and re-layouts, body(): lax.map(partial(block_grads, scaling=head_size ** (-0.5)), inputs)  32.3 us
    all_to_all x1, waiting for transfers between devices, body(): lax.all_to_all(back_values, 'kv', split_axis=0, concat_axis=0, tiled=True)  20 us
    all_to_all x1, waiting for transfers between devices, body(): lax.all_to_all(back_keys, 'kv', split_axis=0, concat_axis=0, tiled=True)  19.8 us
    all_to_all x1, blocking collectives, body(): lax.all_to_all(outgoing_keys, 'kv', split_axis=0, concat_axis=0, tiled=True)  16.8 us
    all_to_all x1, blocking collectives, body(): lax.all_to_all(wanted.reshape(devices, groups), 'kv', split_axis=0, conca...  15.4 us
    unnamed x23, local copies, waits for them, and re-layouts  10.9 us
    while x16, local copies, waits for them, and re-layouts  6.63 us
  transfers between devices with their start and end apart: 5, of which 4 were waited for; matrix products, arithmetic and copies ran while one was open for 8% of the time, Pallas kernels for 0%

commit v1 on v0

--- a/solution.py
+++ b/solution.py
@@ -6,6 +6,28 @@
 
 QB = 128
 KB = 32
+
+
+def split_up(x, dim, size):
+    before, after = (x.shape[:dim], x.shape[dim + 1 :])
+    return jnp.moveaxis(x.reshape(*before, size, -1, *after), dim, 0)
+
+
+def laid_out(tiles, dim):
+    shape = list(tiles.shape[1:])
+    shape[dim] *= tiles.shape[0]
+    return jnp.moveaxis(tiles, 0, dim).reshape(shape)
+
+
+def pairwise_exchange(shard, axis, split_dim, concat_dim):
+    size, here = (lax.axis_size(axis), lax.axis_index(axis))
+    parts = split_up(shard, split_dim, size)
+    done = [parts[here]]
+    for step in range(1, size):
+        sent = parts[here ^ step]
+        done.append(lax.ppermute(sent, axis, [(i, i ^ step) for i in range(size)]))
+    parts = jnp.stack(done)[here ^ jnp.arange(size)]
+    return laid_out(parts, concat_dim)
 
 
 def block_grads(inputs, scaling):
@@ -131,7 +153,7 @@
     back_keys = routed[0, :slot_count].reshape(devices, groups, KB, columns)
     back_values = routed[1, :slot_count].reshape(devices, groups, KB, columns)
     returned_keys, returned_values = (
-        lax.all_to_all(back_keys, "kv", split_axis=0, concat_axis=0, tiled=True),
+        pairwise_exchange(back_keys, "kv", 0, 0),
         lax.all_to_all(back_values, "kv", split_axis=0, concat_axis=0, tiled=True),
     )
     matched = (

time: 305 us -> 306 us (level)
  waiting for transfers between devices: 135 us -> 101 us
  starting transfers between devices: 14.5 us -> 38.9 us
  local copies, waits for them, and re-layouts: 76.8 us -> 87.4 us
    ppermute x0 -> x15, starting transfers between devices: none -> 30 us  [pairwise_exchange(): done.append(lax.ppermute(sent, axis, [(i, i ^ step) for i in range(size)]))]
    all_to_all x1, waiting for transfers between devices: 20 us -> 0.01 us  [body(): lax.all_to_all(back_values, 'kv', split_axis=0, concat_axis=0, tiled=True)]
    all_to_all x1 -> x0, waiting for transfers between devices: 19.8 us -> none  [body(): lax.all_to_all(back_keys, 'kv', split_axis=0, concat_axis=0, tiled=True)]
    ppermute x0 -> x15, waiting for transfers between devices: none -> 7.91 us  [pairwise_exchange(): done.append(lax.ppermute(sent, axis, [(i, i ^ step) for i in range(size)]))]
    unnamed x23 -> x37, local copies, waits for them, and re-layouts: 10.9 us -> 18.2 us
    all_to_all x1 -> x0, starting transfers between devices: 6.09 us -> none  [body(): lax.all_to_all(back_keys, 'kv', split_axis=0, concat_axis=0, tiled=True)]
  transfers between devices with their start and end apart: 5 -> 19, of which waited for: 4 -> 6; matrix products, arithmetic and copies ran while one was open for 8% -> 32% of each run, Pallas kernels for 0% -> 0%
where the time goes in v1:
time: 306 us; the launch traced here: 303 us
  waiting for transfers between devices  101 us (33%)
  local copies, waits for them, and re-layouts  87.4 us (29%)
  starting transfers between devices  38.9 us (13%)
  blocking collectives  32.2 us (11%)
  matrix products  24.7 us (8%)
  between operations  14.4 us (5%)
  other arithmetic  4.54 us (1%)
    reduce_scatter x1, waiting for transfers between devices, body(): lax.psum_scatter(lax.dot_general(features_all, value_grad, (((0,), (0,)),...  89.7 us
    dynamic_update_slice x6, local copies, waits for them, and re-layouts, body(): lax.map(partial(block_grads, scaling=head_size ** (-0.5)), inputs)  32.3 us
    ppermute x15, starting transfers between devices, pairwise_exchange(): done.append(lax.ppermute(sent, axis, [(i, i ^ step) for i in range(size)]))  30 us
    unnamed x37, local copies, waits for them, and re-layouts  18.2 us
    all_to_all x1, blocking collectives, body(): lax.all_to_all(outgoing_keys, 'kv', split_axis=0, concat_axis=0, tiled=True)  16.8 us
    all_to_all x1, blocking collectives, body(): lax.all_to_all(wanted.reshape(devices, groups), 'kv', split_axis=0, conca...  15.4 us
    ppermute x15, waiting for transfers between devices, pairwise_exchange(): done.append(lax.ppermute(sent, axis, [(i, i ^ step) for i in range(size)]))  7.91 us
    while x16, local copies, waits for them, and re-layouts  6.63 us
  transfers between devices with their start and end apart: 19, of which 6 were waited for; matrix products, arithmetic and copies ran while one was open for 32% of the time, Pallas kernels for 0%

profile of v1, /device:TPU:0, one launch (start us, length us, event | category | flops | bytes accessed | tf_op | source)
XLA Modules:
  0.0 303.5 jit_solution(5361922891811265612)
XLA Ops:
  8.1 15.4 %all_to_all.24 = s32[16,1,1]{2,1,0:T(1,128)S(1)} all-to-all(s32[16,1,1]{2,1,0:T(1,128)S(1)} %copy.84), channel_id=1, replica_groups=mesh['kv'=16,'tp'=2] {'kv'}, dimensions={0} | all-to-all | bytes 128 | tf_op jit(solution)/shard_map/all_to_all | solution.py:104
  24.2 1.5 gather_fusion.2
  25.7 1.5 gather_fusion
  27.6 0.9 bitcast_select_fusion
  28.6 16.8 %all_to_all.25 = bf16[16,1,32,512]{3,2,1,0:T(8,128)(2,1)S(1)} all-to-all(bf16[16,1,32,512]{3,2,1,0:T(8,128)(2,1)S(1)} %get-tuple-element.219), channel_id=1, replica_groups=mesh['kv'=16,'tp'=2] {'kv'}, dimensions={0} | all-to-all | bytes 1048576 | tf_op jit(solution)/shard_map/all_to_all | solution.py:119
  45.3 3.8 %all-to-all-start.2 = ((bf16[16,1,32,512]{3,2,1,0:T(8,128)(2,1)}), bf16[16,1,32,512]{3,2,1,0:T(8,128)(2,1)S(1)}, u32[]{:S(2)}, u32[]{:S(2)}) async-start(bf16[16,1,32,512]{3,2,1,0:T(8,128)(2,1)} %get-tuple-element.218), calls=%async_computation.2 | async-start | bytes 1048576 | tf_op jit(solution)/shard_map/all_to_all | solution.py:120
  50.0 1.1 reshape.227
  51.5 1.1 reshape.225
  52.6 1.3 copy.90
  53.9 1.1 reshape.226
  55.0 1.3 copy.91
  56.3 2.0 copy.93
  58.3 1.0 copy.94
  60.7 2.5 all-to-all-done.2
  64.4 56.8 %while.18 = (s32[]{:T(128)}, bf16[2,128,8,64]{1,3,2,0:T(8,128)(2,1)}, f32[2,8,32,8,64]{4,3,2,1,0:T(8,128)}, f32[2,8,32,8,64]{4,3,2,1,0:T(8,128)}, f32[2,128,8,64...) while((s32[]{:T(128)}, ...), condition=%wide.region_3.4_spmd, body=%wide.region_1.3_spmd.sunk | while | flops 306330624 | bytes 43585888 | solution.py:140
  66.1 1.2 fusion.158
  67.3 1.2 fusion.159
  69.2 1.2 fusion.160
  70.4 1.9 fusion.161
  74.6 1.9 copy_dynamic-update-slice_fusion.3
  76.7 1.1 copy-done.3
  78.4 7.1 %dynamic_update_slice.27 = f32[2,128,8,64]{1,0,3,2:T(2,128)} dynamic-update-slice(f32[2,128,8,64]{1,0,3,2:T(2,128)} %get-tuple-element.329, f32[1,128,8,64]{1,0,3,2:T(1,128)S(1)} %bitcast.321, s32[]{:T(128)S(6)} %copy.166, s32[]{:T(128)} %constant.42.clone.1..sunk, s32[]{:T(128)} %constant.42.clone.1..sunk, s32[]{:T(128)} %constant.42.clone.1..sunk) | dynamic-update-slice | bytes 524292 | tf_op jit(solution)/shard_map/while/body/jit(dynamic_update_index_in_dim)/dynamic_update_slice | solution.py:140
  85.8 7.1 %dynamic_update_slice.28 = f32[2,128,8,64]{1,0,3,2:T(2,128)} dynamic-update-slice(f32[2,128,8,64]{1,0,3,2:T(2,128)} %get-tuple-element.330, f32[1,128,8,64]{1,0,3,2:T(1,128)S(1)} %bitcast.320, s32[]{:T(128)S(6)} %copy.166, s32[]{:T(128)} %constant.42.clone.1..sunk, s32[]{:T(128)} %constant.42.clone.1..sunk, s32[]{:T(128)} %constant.42.clone.1..sunk) | dynamic-update-slice | bytes 524292 | tf_op jit(solution)/shard_map/while/body/jit(dynamic_update_index_in_dim)/dynamic_update_slice | solution.py:140
  94.4 1.2 fusion.158
  95.6 1.2 fusion.159
  97.5 1.2 fusion.160
  98.8 1.9 fusion.161
  101.3 0.9 copy-done.5
  102.9 1.9 copy_dynamic-update-slice_fusion.3
  105.0 1.1 copy-done.3
  106.7 7.1 %dynamic_update_slice.27 = f32[2,128,8,64]{1,0,3,2:T(2,128)} dynamic-update-slice(f32[2,128,8,64]{1,0,3,2:T(2,128)} %get-tuple-element.329, f32[1,128,8,64]{1,0,3,2:T(1,128)S(1)} %bitcast.321, s32[]{:T(128)S(6)} %copy.166, s32[]{:T(128)} %constant.42.clone.1..sunk, s32[]{:T(128)} %constant.42.clone.1..sunk, s32[]{:T(128)} %constant.42.clone.1..sunk) | dynamic-update-slice | bytes 524292 | tf_op jit(solution)/shard_map/while/body/jit(dynamic_update_index_in_dim)/dynamic_update_slice | solution.py:140
  114.1 7.1 %dynamic_update_slice.28 = f32[2,128,8,64]{1,0,3,2:T(2,128)} dynamic-update-slice(f32[2,128,8,64]{1,0,3,2:T(2,128)} %get-tuple-element.330, f32[1,128,8,64]{1,0,3,2:T(1,128)S(1)} %bitcast.320, s32[]{:T(128)S(6)} %copy.166, s32[]{:T(128)} %constant.42.clone.1..sunk, s32[]{:T(128)} %constant.42.clone.1..sunk, s32[]{:T(128)} %constant.42.clone.1..sunk) | dynamic-update-slice | bytes 524292 | tf_op jit(solution)/shard_map/while/body/jit(dynamic_update_index_in_dim)/dynamic_update_slice | solution.py:140
  121.2 3.4 %stack_reshape.10 = f32[1,16,16384]{2,1,0:T(8,128)} reshape(f32[2,8,32,8,64]{4,3,2,1,0:T(8,128)} %get-tuple-element.82) | data formatting | bytes 2097152 | tf_op jit(solution)/shard_map/stack;reshape | solution.py:147
  124.6 1.7 stack_reshape.9
  126.2 3.1 %convolution_bitcast_fusion.2 = f32[2,24,16384]{2,1,0:T(8,128)S(1)} fusion(f32[1,16,16384]{2,1,0:T(8,128)} %stack_reshape.10, f32[1,16,16384]{2,1,0:T(8,128)} %stack_reshape.9, s32[16]{0:T(128)S(1)} %eq.46, pred[16]{0:T(512)(128)(4,1)S(1)} %and.45), kind=kOutput, calls=%fused_computation.81 | convolution fusion | flops 151520000 | bytes 5242960 | tf_op jit(solution)/shard_map/ab,xac->xbc/dot_general | solution.py:150
  130.1 0.9 dynamic-slice_bitcast_fusion.1
  131.5 1.6 copy.130
  133.1 4.8 %all-to-all-start.3 = ((f32[16,1,32,512]{3,2,1,0:T(8,128)}), f32[16,1,32,512]{3,2,1,0:T(8,128)}, u32[]{:S(2)}, u32[]{:S(2)}) async-start(f32[16,1,32,512]{3,2,1,0:T(8,128)} %bitcast.322), calls=%async_computation.3 | async-start | bytes 2097152 | tf_op jit(solution)/shard_map/all_to_all | solution.py:157
  138.2 1.9 collective-permute-start.1
  140.1 1.5 collective-permute-start.2
  141.6 1.5 collective-permute-start.3
  143.2 2.8 collective-permute-start.5
  146.0 1.5 bitcast_dynamic-update-slice_fusion.14
  147.4 1.0 collective-permute-done.1
  148.4 1.0 collective-permute-start.6
  150.0 3.6 %collective-permute-start.7 = (f32[1,1,32,512]{3,2,1,0:T(8,128)}, f32[1,1,32,512]{3,2,1,0:T(8,128)S(1)}, u32[]{:S(2)}, u32[]{:S(2)}) collective-permute-start(f32[1,1,32,512]{3,2,1,0:T(8,128)} %get-tuple-element.208), channel_id=1, source_target_pairs={{0,16},{2,18},{4,20},{6,22},{8,24},{10,26},{12,28},{14,30},{16,0},... | collective-permute-start | bytes 196616 | tf_op jit(solution)/shard_map/ppermute | solution.py:28
  154.2 3.2 %collective-permute-done.3 = f32[1,1,32,512]{3,2,1,0:T(8,128)S(1)} collective-permute-done((f32[1,1,32,512]{3,2,1,0:T(8,128)}, f32[1,1,32,512]{3,2,1,0:T(8,128)S(1)}, u32[]{:S(2)}, u32[]{:S(2)}) %collective-permute-start.3) | collective-permute-done | bytes 65568 | tf_op jit(solution)/shard_map/ppermute | solution.py:28
  157.4 5.7 %collective-permute-start.8 = (f32[1,1,32,512]{3,2,1,0:T(8,128)}, f32[1,1,32,512]{3,2,1,0:T(8,128)S(1)}, u32[]{:S(2)}, u32[]{:S(2)}) collective-permute-start(f32[1,1,32,512]{3,2,1,0:T(8,128)} %get-tuple-element.207), channel_id=1, source_target_pairs={{0,18},{2,16},{4,22},{6,20},{8,26},{10,24},{12,30},{14,28},{16,2},... | collective-permute-start | bytes 196616 | tf_op jit(solution)/shard_map/ppermute | solution.py:28
  163.7 1.7 collective-permute-start.9
  166.1 2.2 collective-permute-start.10
  169.5 2.0 collective-permute-done.7
  171.5 2.6 collective-permute-start.12
  174.8 1.8 collective-permute-start.13
  177.2 3.1 %collective-permute-start.14 = (f32[1,1,32,512]{3,2,1,0:T(8,128)S(1)}, f32[1,1,32,512]{3,2,1,0:T(8,128)S(1)}, u32[]{:S(2)}, u32[]{:S(2)}) collective-permute-start(f32[1,1,32,512]{3,2,1,0:T(8,128)S(1)} %get-tuple-element.201), channel_id=1, source_target_pairs={{0,30},{2,28},{4,26},{6,24},{8,22},{10,20},{12,18},{14,16},{16,14}... | collective-permute-start | bytes 196616 | tf_op jit(solution)/shard_map/ppermute | solution.py:28
  183.4 1.8 collective-permute-done.14
  185.7 2.8 gather_fusion.4
  188.5 2.4 stack_reshape_reshape.3
  191.0 2.4 stack_reshape.11
  193.3 2.3 fusion.59
  196.8 3.9 %convolution_bitcast_fusion.4 = f32[2048,512]{0,1:T(8,128)} fusion(bf16[256,512]{0,1:T(8,128)(2,1)S(1)} %fusion.66, bf16[256,2048]{1,0:T(8,128)(2,1)} %all-gather.2.cloned.1.call-done), kind=kOutput, calls=%fused_computation.84 | convolution fusion | flops 536870912 | bytes 5505024 | tf_op jit(solution)/shard_map/dot_general | solution.py:179
  200.7 1.3 copy.117
  202.1 1.0 reshape.229
  205.2 89.7 %reduce-scatter.2.cloned.1.call-done = f32[128,512]{0,1:T(8,128)} async-done(((f32[2048,512]{0,1:T(8,128)}), f32[128,512]{0,1:T(8,128)}) %reduce-scatter.2.cloned.1.call-update) | async-done | bytes 262160 | tf_op jit(solution)/shard_map/reduce_scatter | solution.py:178
  294.9 1.8 copy.106
  (136 shorter events, 29.1 us)
Async XLA Ops:
  27.6 22.3 %copy-start.1 = (bf16[256,512]{1,0:T(8,128)(2,1)S(1)}, bf16[256,512]{1,0:T(8,128)(2,1)}, u32[]{:S(2)}) copy-start(bf16[256,512]{1,0:T(8,128)(2,1)} %param.11) | copy-start | bytes 786436
  28.6 22.5 %copy-start = (bf16[256,512]{1,0:T(8,128)(2,1)S(1)}, bf16[256,512]{1,0:T(8,128)(2,1)}, u32[]{:S(2)}) copy-start(bf16[256,512]{1,0:T(8,128)(2,1)} %param.10) | copy-start | bytes 786436
  28.6 22.9 %copy-start.9 = (bf16[256,512]{1,0:T(8,128)(2,1)S(1)}, bf16[256,512]{1,0:T(8,128)(2,1)}, u32[]{:S(2)}) copy-start(bf16[256,512]{1,0:T(8,128)(2,1)} %param.9) | copy-start | bytes 786436
  45.3 17.8 %all-to-all-start.2 = ((bf16[16,1,32,512]{3,2,1,0:T(8,128)(2,1)}), bf16[16,1,32,512]{3,2,1,0:T(8,128)(2,1)S(1)}, u32[]{:S(2)}, u32[]{:S(2)}) async-start(bf16[16,1,32,512]{3,2,1,0:T(8,128)(2,1)} %get-tuple-element.218), calls=%async_computation.2 | async-start | bytes 1048576 | tf_op jit(solution)/shard_map/all_to_all | solution.py:120
  49.2 4.7 %copy-start.10 = (bf16[256,512]{1,0:T(8,128)(2,1)S(1)}, bf16[256,512]{1,0:T(8,128)(2,1)}, u32[]{:S(2)}) copy-start(bf16[256,512]{1,0:T(8,128)(2,1)} %param.13) | copy-start | bytes 786436
  49.2 147.6 %all-gather.2.cloned.1.call-start = ((), (), s32[]{:S(2)}) async-start(), calls=%async_computation.5 | async-start | bytes 1572864 | tf_op jit(solution)/shard_map/all_gather | solution.py:177
  63.2 1.2 copy-start.11
  72.3 1.6 copy-start.5
  72.6 2.0 copy-start.2
  76.5 1.3 copy-start.3
  76.5 1.9 copy-start.6
  100.6 1.6 copy-start.5
  100.9 2.0 copy-start.2
  104.8 1.3 copy-start.3
  104.8 1.9 copy-start.6
  121.2 3.4 %copy-start.4 = (f32[2,8,32,8,64]{4,3,2,1,0:T(8,128)S(1)}, f32[2,8,32,8,64]{4,3,2,1,0:T(8,128)}, u32[]{:S(2)}) copy-start(f32[2,8,32,8,64]{4,3,2,1,0:T(8,128)} %get-tuple-element.81) | copy-start | bytes 3145732
  131.0 12.2 %collective-permute-start = (f32[1,1,32,512]{3,2,1,0:T(8,128)}, f32[1,1,32,512]{3,2,1,0:T(8,128)}, u32[]{:S(2)}, u32[]{:S(2)}) collective-permute-start(f32[1,1,32,512]{3,2,1,0:T(8,128)} %get-tuple-element.215), channel_id=1, source_target_pairs={{0,2},{2,0},{4,6},{6,4},{8,10},{10,8},{12,14},{14,12},{16,18},{18,... | collective-permute-start | bytes 196616 | tf_op jit(solution)/shard_map/ppermute | solution.py:28
  133.1 57.9 %all-to-all-start.3 = ((f32[16,1,32,512]{3,2,1,0:T(8,128)}), f32[16,1,32,512]{3,2,1,0:T(8,128)}, u32[]{:S(2)}, u32[]{:S(2)}) async-start(f32[16,1,32,512]{3,2,1,0:T(8,128)} %bitcast.322), calls=%async_computation.3 | async-start | bytes 2097152 | tf_op jit(solution)/shard_map/all_to_all | solution.py:157
  137.9 157.0 %reduce-scatter.2.cloned.1.call-start = ((), (), s32[]{:S(2)}) async-start(), calls=%async_computation.6 | async-start | bytes 4456448 | tf_op jit(solution)/shard_map/reduce_scatter | solution.py:178
  138.2 10.2 %collective-permute-start.1 = (f32[1,1,32,512]{3,2,1,0:T(8,128)}, f32[1,1,32,512]{3,2,1,0:T(8,128)S(1)}, u32[]{:S(2)}, u32[]{:S(2)}) collective-permute-start(f32[1,1,32,512]{3,2,1,0:T(8,128)} %get-tuple-element.214), channel_id=1, source_target_pairs={{0,4},{2,6},{4,0},{6,2},{8,12},{10,14},{12,8},{14,10},{16,20},{18,... | collective-permute-start | bytes 196616 | tf_op jit(solution)/shard_map/ppermute | solution.py:28
  140.1 9.9 %collective-permute-start.2 = (f32[1,1,32,512]{3,2,1,0:T(8,128)}, f32[1,1,32,512]{3,2,1,0:T(8,128)S(1)}, u32[]{:S(2)}, u32[]{:S(2)}) collective-permute-start(f32[1,1,32,512]{3,2,1,0:T(8,128)} %get-tuple-element.213), channel_id=1, source_target_pairs={{0,6},{2,4},{4,2},{6,0},{8,14},{10,12},{12,10},{14,8},{16,22},{18,... | collective-permute-start | bytes 196616 | tf_op jit(solution)/shard_map/ppermute | solution.py:28
  141.6 15.8 %collective-permute-start.3 = (f32[1,1,32,512]{3,2,1,0:T(8,128)}, f32[1,1,32,512]{3,2,1,0:T(8,128)S(1)}, u32[]{:S(2)}, u32[]{:S(2)}) collective-permute-start(f32[1,1,32,512]{3,2,1,0:T(8,128)} %get-tuple-element.212), channel_id=1, source_target_pairs={{0,8},{2,10},{4,12},{6,14},{8,0},{10,2},{12,4},{14,6},{16,24},{18,... | collective-permute-start | bytes 196616 | tf_op jit(solution)/shard_map/ppermute | solution.py:28
  143.0 20.7 %collective-permute-start.4 = (f32[1,1,32,512]{3,2,1,0:T(8,128)}, f32[1,1,32,512]{3,2,1,0:T(8,128)S(1)}, u32[]{:S(2)}, u32[]{:S(2)}) collective-permute-start(f32[1,1,32,512]{3,2,1,0:T(8,128)} %get-tuple-element.211), channel_id=1, source_target_pairs={{0,10},{2,8},{4,14},{6,12},{8,2},{10,0},{12,6},{14,4},{16,26},{18,... | collective-permute-start | bytes 196616 | tf_op jit(solution)/shard_map/ppermute | solution.py:28
  143.2 22.9 %collective-permute-start.5 = (f32[1,1,32,512]{3,2,1,0:T(8,128)}, f32[1,1,32,512]{3,2,1,0:T(8,128)S(1)}, u32[]{:S(2)}, u32[]{:S(2)}) collective-permute-start(f32[1,1,32,512]{3,2,1,0:T(8,128)} %get-tuple-element.210), channel_id=1, source_target_pairs={{0,12},{2,14},{4,8},{6,10},{8,4},{10,6},{12,0},{14,2},{16,28},{18,... | collective-permute-start | bytes 196616 | tf_op jit(solution)/shard_map/ppermute | solution.py:28
  148.4 20.5 %collective-permute-start.6 = (f32[1,1,32,512]{3,2,1,0:T(8,128)}, f32[1,1,32,512]{3,2,1,0:T(8,128)S(1)}, u32[]{:S(2)}, u32[]{:S(2)}) collective-permute-start(f32[1,1,32,512]{3,2,1,0:T(8,128)} %get-tuple-element.209), channel_id=1, source_target_pairs={{0,14},{2,12},{4,10},{6,8},{8,6},{10,4},{12,2},{14,0},{16,30},{18,... | collective-permute-start | bytes 196616 | tf_op jit(solution)/shard_map/ppermute | solution.py:28
  150.0 21.5 %collective-permute-start.7 = (f32[1,1,32,512]{3,2,1,0:T(8,128)}, f32[1,1,32,512]{3,2,1,0:T(8,128)S(1)}, u32[]{:S(2)}, u32[]{:S(2)}) collective-permute-start(f32[1,1,32,512]{3,2,1,0:T(8,128)} %get-tuple-element.208), channel_id=1, source_target_pairs={{0,16},{2,18},{4,20},{6,22},{8,24},{10,26},{12,28},{14,30},{16,0},... | collective-permute-start | bytes 196616 | tf_op jit(solution)/shard_map/ppermute | solution.py:28
  157.4 17.4 %collective-permute-start.8 = (f32[1,1,32,512]{3,2,1,0:T(8,128)}, f32[1,1,32,512]{3,2,1,0:T(8,128)S(1)}, u32[]{:S(2)}, u32[]{:S(2)}) collective-permute-start(f32[1,1,32,512]{3,2,1,0:T(8,128)} %get-tuple-element.207), channel_id=1, source_target_pairs={{0,18},{2,16},{4,22},{6,20},{8,26},{10,24},{12,30},{14,28},{16,2},... | collective-permute-start | bytes 196616 | tf_op jit(solution)/shard_map/ppermute | solution.py:28
  163.7 13.5 %collective-permute-start.9 = (f32[1,1,32,512]{3,2,1,0:T(8,128)S(1)}, f32[1,1,32,512]{3,2,1,0:T(8,128)S(1)}, u32[]{:S(2)}, u32[]{:S(2)}) collective-permute-start(f32[1,1,32,512]{3,2,1,0:T(8,128)S(1)} %get-tuple-element.206), channel_id=1, source_target_pairs={{0,20},{2,22},{4,16},{6,18},{8,28},{10,30},{12,24},{14,26},{16,4},... | collective-permute-start | bytes 196616 | tf_op jit(solution)/shard_map/ppermute | solution.py:28
  166.1 14.8 %collective-permute-start.10 = (f32[1,1,32,512]{3,2,1,0:T(8,128)S(1)}, f32[1,1,32,512]{3,2,1,0:T(8,128)S(1)}, u32[]{:S(2)}, u32[]{:S(2)}) collective-permute-start(f32[1,1,32,512]{3,2,1,0:T(8,128)S(1)} %get-tuple-element.205), channel_id=1, source_target_pairs={{0,22},{2,20},{4,18},{6,16},{8,30},{10,28},{12,26},{14,24},{16,6},... | collective-permute-start | bytes 196616 | tf_op jit(solution)/shard_map/ppermute | solution.py:28
  168.9 12.6 %collective-permute-start.11 = (f32[1,1,32,512]{3,2,1,0:T(8,128)S(1)}, f32[1,1,32,512]{3,2,1,0:T(8,128)S(1)}, u32[]{:S(2)}, u32[]{:S(2)}) collective-permute-start(f32[1,1,32,512]{3,2,1,0:T(8,128)S(1)} %get-tuple-element.204), channel_id=1, source_target_pairs={{0,24},{2,26},{4,28},{6,30},{8,16},{10,18},{12,20},{14,22},{16,8},... | collective-permute-start | bytes 196616 | tf_op jit(solution)/shard_map/ppermute | solution.py:28
  171.5 10.6 %collective-permute-start.12 = (f32[1,1,32,512]{3,2,1,0:T(8,128)S(1)}, f32[1,1,32,512]{3,2,1,0:T(8,128)S(1)}, u32[]{:S(2)}, u32[]{:S(2)}) collective-permute-start(f32[1,1,32,512]{3,2,1,0:T(8,128)S(1)} %get-tuple-element.203), channel_id=1, source_target_pairs={{0,26},{2,24},{4,30},{6,28},{8,18},{10,16},{12,22},{14,20},{16,10}... | collective-permute-start | bytes 196616 | tf_op jit(solution)/shard_map/ppermute | solution.py:28
  174.8 8.0 %collective-permute-start.13 = (f32[1,1,32,512]{3,2,1,0:T(8,128)S(1)}, f32[1,1,32,512]{3,2,1,0:T(8,128)S(1)}, u32[]{:S(2)}, u32[]{:S(2)}) collective-permute-start(f32[1,1,32,512]{3,2,1,0:T(8,128)S(1)} %get-tuple-element.202), channel_id=1, source_target_pairs={{0,28},{2,30},{4,24},{6,26},{8,20},{10,22},{12,16},{14,18},{16,12}... | collective-permute-start | bytes 196616 | tf_op jit(solution)/shard_map/ppermute | solution.py:28
  177.2 8.0 %collective-permute-start.14 = (f32[1,1,32,512]{3,2,1,0:T(8,128)S(1)}, f32[1,1,32,512]{3,2,1,0:T(8,128)S(1)}, u32[]{:S(2)}, u32[]{:S(2)}) collective-permute-start(f32[1,1,32,512]{3,2,1,0:T(8,128)S(1)} %get-tuple-element.201), channel_id=1, source_target_pairs={{0,30},{2,28},{4,26},{6,24},{8,22},{10,20},{12,18},{14,16},{16,14}... | collective-permute-start | bytes 196616 | tf_op jit(solution)/shard_map/ppermute | solution.py:28
  195.7 1.0 copy-start.8
  200.7 3.5 %copy-start.7 = (f32[2,128,8,64]{1,0,3,2:T(2,128)S(1)}, f32[2,128,8,64]{1,0,3,2:T(2,128)}, u32[]{:S(2)}) copy-start(f32[2,128,8,64]{1,0,3,2:T(2,128)} %get-tuple-element.83) | copy-start | bytes 1572868
Sparse Core Ops, SparseCore 0:
  51.5 10.3 all-gather.1
  200.9 93.9 reduce-scatter.1
